TPU v7x, 32 devices: a whole 2x2x4 slice. The times are simulated.
32 devices in a mesh: grp: 2 (over y), ra: 4 (over z), cb: 4 (over x, core).
Axes of the slice: x: 2, y: 2, z: 4, core: 2. Of those that a mesh axis runs over, the one named last changes fastest.
Arguments:
- tokens: bfloat16 [512, 4096], P('grp', 'ra'), parts along dimension 0, may hold values from -30 to 30, as said below
- norm_gain: bfloat16 [4096], P('ra'), may hold values from 0.099609375 to 1.8984375
- w_gate: bfloat16 [4096, 11264], P('ra', 'cb'), may hold values from -0.09375 to 0.09375
- w_value: bfloat16 [4096, 11264], P('ra', 'cb'), may hold values from -0.09375 to 0.09375
- conv_gate: float32 [3, 11264], P(None, 'cb'), may hold values from -3 to 3
- conv_value: float32 [3, 11264], P(None, 'cb'), may hold values from -3 to 3
- bias_gate: float32 [11264], P('cb'), may hold values from -3 to 3
- bias_value: float32 [11264], P('cb'), may hold values from -3 to 3
- w_down: bfloat16 [11264, 4096], P('cb', 'ra'), may hold values from -1 to 1
- out_gain: bfloat16 [4096], P('ra'), may hold values from 0.099609375 to 1.8984375
Outputs:
- normed_out: bfloat16 [512, 4096], P('grp', 'ra'), parts along dimension 0
There are 2 independent parts, one for each index of `grp`. A program takes and returns all parts, laid end to end along the dimension named above; an argument that names none is the same for every part. Nothing has to cross between parts.
Inputs may be any that keep to these rules, and one draw needn't show every extreme that they name: `tokens`: feature scales differ along the width.
All inputs are finite; a program needn't handle non-finite values.
Results may differ from a plain program's by a relative error of at most 0.0059.
Values may be sent and summed in bfloat16 or wider, within the bound.
A program may use at most 64 MiB of HBM per device.

v0:
```python
import jax
import jax.numpy as jnp
from jax import lax
from jax.sharding import PartitionSpec as P

EPSILON = 1e-06
RESIDUAL_WEIGHT = 0.25


def spread(signal, kernel):
    padded = jnp.pad(signal, ((1, 1), (0, 0)))
    return padded[:-2] * kernel[0] + padded[1:-1] * kernel[1] + padded[2:] * kernel[2]


def activate(gate_sum, value_sum, kernel_gate, kernel_value, offset_gate, offset_value):
    gate_conv = spread(gate_sum, kernel_gate) + offset_gate
    value_conv = spread(value_sum, kernel_value) + offset_value
    return (jax.nn.silu(gate_conv) * value_conv).astype(jnp.bfloat16)


def body(
    tokens,
    norm_gain,
    w_gate,
    w_value,
    conv_gate,
    conv_value,
    bias_gate,
    bias_value,
    w_down,
    out_gain,
):
    wide_in = tokens.astype(jnp.float32)
    width = wide_in.shape[1] * lax.axis_size("ra")
    squares = lax.psum(jnp.sum(wide_in * wide_in, axis=1), "ra")
    rscale = lax.rsqrt(squares / width + EPSILON)
    normed = (wide_in * rscale[:, None] * norm_gain.astype(jnp.float32)).astype(jnp.bfloat16)
    part_gate = jnp.dot(normed, w_gate, preferred_element_type=jnp.float32)
    part_value = jnp.dot(normed, w_value, preferred_element_type=jnp.float32)
    gate_sum, value_sum = (
        lax.psum_scatter(part_gate, "ra", scatter_dimension=1, tiled=True),
        lax.psum_scatter(part_value, "ra", scatter_dimension=1, tiled=True),
    )
    share_cols = gate_sum.shape[1]
    first_col = lax.axis_index("ra") * share_cols
    local_hidden = activate(
        gate_sum,
        value_sum,
        lax.dynamic_slice_in_dim(conv_gate, first_col, share_cols, 1),
        lax.dynamic_slice_in_dim(conv_value, first_col, share_cols, 1),
        lax.dynamic_slice_in_dim(bias_gate, first_col, share_cols, 0),
        lax.dynamic_slice_in_dim(bias_value, first_col, share_cols, 0),
    )
    partial_value = jnp.dot(
        lax.all_gather(local_hidden, "ra", axis=1, tiled=True),
        w_down,
        preferred_element_type=jnp.float32,
    )
    branch = lax.psum(partial_value, "cb")
    summed = RESIDUAL_WEIGHT * wide_in + branch
    totals = lax.psum(jnp.sum(summed * summed, axis=1), "ra")
    oscale = lax.rsqrt(totals / width + EPSILON)
    return (summed * oscale[:, None] * out_gain.astype(jnp.float32)).astype(jnp.bfloat16)


def solution(mesh):
    return jax.shard_map(
        body,
        mesh=mesh,
        in_specs=(
            P("grp", "ra"),
            P("ra"),
            P("ra", "cb"),
            P("ra", "cb"),
            P(None, "cb"),
            P(None, "cb"),
            P("cb"),
            P("cb"),
            P("cb", "ra"),
            P("ra"),
        ),
        out_specs=P("grp", "ra"),
        check_vma=False,
    )
```

profile of v0, /device:TPU:0, one launch (start us, length us, event | category | flops | bytes accessed | tf_op | source)
XLA Modules:
  0.0 244.4 jit_solution(13220206293900376885)
XLA Ops:
  6.5 0.7 convert_element_type.22
  7.2 1.2 fusion.1
  8.4 13.5 %psum.21 = f32[256]{0:T(256)S(1)} all-reduce(f32[256]{0:T(256)S(1)} %fusion.1), channel_id=1, replica_groups=mesh['grp'=2,'ra'=4,'cb'=4] {'ra'}, use_global_device_ids=true, to_apply=%region_1.0 | all-reduce | flops 256 | bytes 2048 | tf_op jit(solution)/shard_map/psum | solution.py:35
  21.9 6.9 %fusion.16 = f32[256,2816]{0,1:T(8,128)} fusion(bf16[1024,2816]{1,0:T(8,128)(2,1)} %param.13, bf16[256,1024]{1,0:T(8,128)(2,1)} %param.10, f32[1024]{0:T(1024)S(1)} %convert_element_type.22, f32[256]{0:T(256)S(1)} %add_rsqrt_fusion.1), kind=kOutput, calls=%fused_computation.25 | convolution fusion | flops 1477443584 | bytes 9180160 | tf_op jit(solution)/shard_map/dot_general | solution.py:39
  28.8 0.0 reduce-scatter.5.cloned.1.call-update
  28.8 0.0 reduce-scatter.3.cloned.1.call-start
  28.9 6.7 %fusion.18 = f32[256,2816]{0,1:T(8,128)} fusion(bf16[1024,2816]{1,0:T(8,128)(2,1)} %param.12, bf16[256,1024]{1,0:T(8,128)(2,1)S(1)} %copy-done, f32[1024]{0:T(1024)S(1)} %convert_element_type.22, f32[256]{0:T(256)S(1)} %add_rsqrt_fusion.1), kind=kOutput, calls=%fused_computation.26 | convolution fusion | flops 1477443584 | bytes 9180160 | tf_op jit(solution)/shard_map/dot_general | solution.py:38
  35.5 0.0 reduce-scatter.3.cloned.1.call-update
  35.6 0.0 all-gather.2.cloned.1.call-start
  35.6 0.8 dynamic_slice.15
  36.4 0.8 dynamic_slice.13
  37.2 0.9 dynamic-slice_reduce_fusion.2
  38.1 45.4 %reduce-scatter.5.cloned.1.call-done = f32[256,704]{0,1:T(8,128)} async-done(((f32[256,2816]{0,1:T(8,128)}), f32[256,704]{0,1:T(8,128)}) %reduce-scatter.5.cloned.1.call-update) | async-done | bytes 720912 | tf_op jit(solution)/shard_map/reduce_scatter | solution.py:42
  83.5 58.4 %reduce-scatter.3.cloned.1.call-done = f32[256,704]{0,1:T(8,128)} async-done(((f32[256,2816]{0,1:T(8,128)}), f32[256,704]{0,1:T(8,128)}) %reduce-scatter.3.cloned.1.call-update) | async-done | bytes 720912 | tf_op jit(solution)/shard_map/reduce_scatter | solution.py:41
  141.9 4.6 %fusion.14 = bf16[256,704]{0,1:T(8,128)(2,1)} fusion(f32[256,704]{0,1:T(8,128)} %reduce-scatter.5.cloned.1.call-done, f32[256,704]{0,1:T(8,128)} %reduce-scatter.3.cloned.1.call-done, f32[704]{0:T(1024)S(1)} %dynamic_slice.15, f32[704]{0:T(1024)S(1)} %get-tuple-element.10, f32[704]{0:T(1024)S(1)} %get-tuple-element.9, f32[704]{0:T(1024)S(1)} %get-tuple-element.8, ...), kind=kLoop, calls=%fused_computation.23 | loop fusion | flops 3244032 | bytes 1824768 | tf_op jit(solution)/shard_map/convert_element_type | solution.py:18
  146.6 0.0 all-gather.2.cloned.1.call-update
  146.6 0.0 all-reduce.4.cloned.1.call-start
  146.6 34.6 %all-gather.2.cloned.1.call-done = bf16[256,2816]{0,1:T(8,128)(2,1)} async-done(((bf16[256,704]{0,1:T(8,128)(2,1)}), bf16[256,2816]{0,1:T(8,128)(2,1)}) %all-gather.2.cloned.1.call-update) | async-done | bytes 1441808 | tf_op jit(solution)/shard_map/all_gather | solution.py:55
  181.2 5.7 %fusion.20 = f32[256,1024]{1,0:T(8,128)} fusion(bf16[256,2816]{0,1:T(8,128)(2,1)} %all-gather.2.cloned.1.call-done, bf16[2816,1024]{1,0:T(8,128)(2,1)} %param.18), kind=kOutput, calls=%fused_computation.35 | convolution fusion | flops 1476395008 | bytes 8257536 | tf_op jit(solution)/shard_map/dot_general | solution.py:54
  187.0 0.0 all-reduce.4.cloned.1.call-update
  187.0 35.4 %all-reduce.4.cloned.1.call-done = f32[256,1024]{1,0:T(8,128)} async-done(((f32[256,1024]{1,0:T(8,128)}), f32[256,1024]{1,0:T(8,128)}) %all-reduce.4.cloned.1.call-update) | async-done | bytes 1048592 | tf_op jit(solution)/shard_map/psum | solution.py:59
  222.4 1.5 multiply_reduce_fusion
  223.9 11.7 %psum.23 = f32[256]{0:T(256)S(1)} all-reduce(f32[256]{0:T(256)S(1)} %multiply_reduce_fusion), channel_id=1, replica_groups=mesh['grp'=2,'ra'=4,'cb'=4] {'ra'}, use_global_device_ids=true, to_apply=%region_6.7 | all-reduce | flops 256 | bytes 2048 | tf_op jit(solution)/shard_map/psum | solution.py:61
  235.6 2.2 multiply_convert_fusion
  (8 shorter events, 0.0 us)
Async XLA Ops:
  6.5 77.0 %reduce-scatter.5.cloned.1.call-start = ((), (), s32[]{:S(2)}) async-start(), calls=%async_computation.3 | async-start | bytes 3604480 | tf_op jit(solution)/shard_map/reduce_scatter | solution.py:42
  21.9 6.9 %copy-start = (bf16[256,1024]{1,0:T(8,128)(2,1)S(1)}, bf16[256,1024]{1,0:T(8,128)(2,1)}, u32[]{:S(2)}) copy-start(bf16[256,1024]{1,0:T(8,128)(2,1)} %param.10) | copy-start | bytes 1572868
  28.8 113.1 %reduce-scatter.3.cloned.1.call-start = ((), (), s32[]{:S(2)}) async-start(), calls=%async_computation.2 | async-start | bytes 3604480 | tf_op jit(solution)/shard_map/reduce_scatter | solution.py:41
  35.6 145.7 %all-gather.2.cloned.1.call-start = ((), (), s32[]{:S(2)}) async-start(), calls=%async_computation.4 | async-start | bytes 1802240 | tf_op jit(solution)/shard_map/all_gather | solution.py:55
  146.6 40.4 %copy-start.1 = (bf16[1024]{0:T(1024)(128)(2,1)S(1)}, bf16[1024]{0:T(1024)(128)(2,1)}, u32[]{:S(2)}) copy-start(bf16[1024]{0:T(1024)(128)(2,1)} %param.19) | copy-start | bytes 6148
  146.6 75.8 %all-reduce.4.cloned.1.call-start = ((), (), s32[]{:S(2)}) async-start(), calls=%async_computation.5 | async-start | bytes 2097152 | tf_op jit(solution)/shard_map/psum | solution.py:59
Sparse Core Ops, SparseCore 0:
  28.9 54.5 reduce-scatter.4
  85.8 56.0 reduce-scatter.2
  146.7 34.4 all-gather.1
  187.1 35.2 all-reduce.3
where the time goes:
time: 245 us; the launch traced here: 244 us
  waiting for transfers between devices  174 us (71%)
  blocking collectives  25.2 us (10%)
  matrix products  19.3 us (8%)
  between operations  13.2 us (5%)
  other arithmetic  10.3 us (4%)
  local copies, waits for them, and re-layouts  2.5 us (1%)
    reduce_scatter x1, waiting for transfers between devices, body(): lax.psum_scatter(part_gate, 'ra', scatter_dimension=1, tiled=True)  58.4 us
    reduce_scatter x1, waiting for transfers between devices, body(): lax.psum_scatter(part_value, 'ra', scatter_dimension=1, tiled=True)  45.4 us
    psum x1, waiting for transfers between devices, body(): branch = lax.psum(partial_value, 'cb')  35.4 us
    all_gather x1, waiting for transfers between devices, body(): lax.all_gather(local_hidden, 'ra', axis=1, tiled=True)  34.6 us
    psum x1, blocking collectives, body(): squares = lax.psum(jnp.sum(wide_in * wide_in, axis=1), 'ra')  13.5 us
    psum x1, blocking collectives, body(): totals = lax.psum(jnp.sum(summed * summed, axis=1), 'ra')  11.7 us
    dot_general x1, matrix products, body(): part_value = jnp.dot(normed, w_value, preferred_element_type=jnp.float32)  6.85 us
    dot_general x1, matrix products, body(): part_gate = jnp.dot(normed, w_gate, preferred_element_type=jnp.float32)  6.67 us
  transfers between devices with their start and end apart: 4, of which 4 were waited for; matrix products, arithmetic and copies ran while one was open for 4% of the time, Pallas kernels for 0%

commit v1 on v0

--- a/solution.py
+++ b/solution.py
@@ -5,6 +5,12 @@
 
 EPSILON = 1e-06
 RESIDUAL_WEIGHT = 0.25
+
+
+def gather_blocks(block, mesh_axis, along):
+    pieces = lax.all_gather(block, mesh_axis, axis=0, tiled=False)
+    result = jnp.concatenate(pieces, axis=along)
+    return result
 
 
 def spread(signal, kernel):
@@ -52,9 +58,7 @@
         lax.dynamic_slice_in_dim(bias_value, first_col, share_cols, 0),
     )
     partial_value = jnp.dot(
-        lax.all_gather(local_hidden, "ra", axis=1, tiled=True),
-        w_down,
-        preferred_element_type=jnp.float32,
+        gather_blocks(local_hidden, "ra", 1), w_down, preferred_element_type=jnp.float32
     )
     branch = lax.psum(partial_value, "cb")
     summed = RESIDUAL_WEIGHT * wide_in + branch

time: 245 us -> 246 us (level)
  no operation moved by 1% of the time
where the time goes in v1:
time: 246 us; the launch traced here: 245 us
  waiting for transfers between devices  174 us (71%)
  blocking collectives  25.2 us (10%)
  matrix products  18.9 us (8%)
  between operations  13.2 us (5%)
  other arithmetic  10.3 us (4%)
  local copies, waits for them, and re-layouts  3.95 us (2%)
    reduce_scatter x1, waiting for transfers between devices, body(): lax.psum_scatter(part_gate, 'ra', scatter_dimension=1, tiled=True)  58.4 us
    reduce_scatter x1, waiting for transfers between devices, body(): lax.psum_scatter(part_value, 'ra', scatter_dimension=1, tiled=True)  45.4 us
    all_gather x1, waiting for transfers between devices, gather_blocks(): pieces = lax.all_gather(block, mesh_axis, axis=0, tiled=False)  35.4 us
    psum x1, waiting for transfers between devices, body(): branch = lax.psum(partial_value, 'cb')  34.6 us
    psum x1, blocking collectives, body(): squares = lax.psum(jnp.sum(wide_in * wide_in, axis=1), 'ra')  13.5 us
    psum x1, blocking collectives, body(): totals = lax.psum(jnp.sum(summed * summed, axis=1), 'ra')  11.7 us
    dot_general x1, matrix products, body(): part_value = jnp.dot(normed, w_value, preferred_element_type=jnp.float32)  6.85 us
    dot_general x1, matrix products, body(): part_gate = jnp.dot(normed, w_gate, preferred_element_type=jnp.float32)  6.67 us
  transfers between devices with their start and end apart: 4, of which 4 were waited for; matrix products, arithmetic and copies ran while one was open for 4% of the time, Pallas kernels for 0%

profile of v1, /device:TPU:0, one launch (start us, length us, event | category | flops | bytes accessed | tf_op | source)
XLA Modules:
  0.0 245.5 jit_solution(17280826574055454875)
XLA Ops:
  6.5 0.7 convert_element_type.22
  7.2 1.2 fusion.1
  8.4 13.5 %psum.21 = f32[256]{0:T(256)S(1)} all-reduce(f32[256]{0:T(256)S(1)} %fusion.1), channel_id=1, replica_groups=mesh['grp'=2,'ra'=4,'cb'=4] {'ra'}, use_global_device_ids=true, to_apply=%region_1.0 | all-reduce | flops 256 | bytes 2048 | tf_op jit(solution)/shard_map/psum | solution.py:41
  21.9 6.9 %fusion.16 = f32[256,2816]{0,1:T(8,128)} fusion(bf16[1024,2816]{1,0:T(8,128)(2,1)} %param.13, bf16[256,1024]{1,0:T(8,128)(2,1)} %param.10, f32[1024]{0:T(1024)S(1)} %convert_element_type.22, f32[256]{0:T(256)S(1)} %add_rsqrt_fusion.1), kind=kOutput, calls=%fused_computation.26 | convolution fusion | flops 1477443584 | bytes 9180160 | tf_op jit(solution)/shard_map/dot_general | solution.py:45
  28.8 0.0 reduce-scatter.5.cloned.1.call-update
  28.8 0.0 reduce-scatter.3.cloned.1.call-start
  28.9 6.7 %fusion.18 = f32[256,2816]{0,1:T(8,128)} fusion(bf16[1024,2816]{1,0:T(8,128)(2,1)} %param.12, bf16[256,1024]{1,0:T(8,128)(2,1)S(1)} %copy-done, f32[1024]{0:T(1024)S(1)} %convert_element_type.22, f32[256]{0:T(256)S(1)} %add_rsqrt_fusion.1), kind=kOutput, calls=%fused_computation.27 | convolution fusion | flops 1477443584 | bytes 9180160 | tf_op jit(solution)/shard_map/dot_general | solution.py:44
  35.6 0.0 all-gather.3.cloned.1.call-start
  35.6 0.8 dynamic_slice.15
  36.4 0.8 dynamic_slice.13
  37.2 0.9 dynamic-slice_reduce_fusion.2
  38.1 45.4 %reduce-scatter.5.cloned.1.call-done = f32[256,704]{0,1:T(8,128)} async-done(((f32[256,2816]{0,1:T(8,128)}), f32[256,704]{0,1:T(8,128)}) %reduce-scatter.5.cloned.1.call-update) | async-done | bytes 720912 | tf_op jit(solution)/shard_map/reduce_scatter | solution.py:48
  83.5 58.4 %reduce-scatter.3.cloned.1.call-done = f32[256,704]{0,1:T(8,128)} async-done(((f32[256,2816]{0,1:T(8,128)}), f32[256,704]{0,1:T(8,128)}) %reduce-scatter.3.cloned.1.call-update) | async-done | bytes 720912 | tf_op jit(solution)/shard_map/reduce_scatter | solution.py:47
  141.9 4.6 %fusion.14 = bf16[256,704]{0,1:T(8,128)(2,1)} fusion(f32[256,704]{0,1:T(8,128)} %reduce-scatter.5.cloned.1.call-done, f32[256,704]{0,1:T(8,128)} %reduce-scatter.3.cloned.1.call-done, f32[704]{0:T(1024)S(1)} %dynamic_slice.15, f32[704]{0:T(1024)S(1)} %get-tuple-element.10, f32[704]{0:T(1024)S(1)} %get-tuple-element.9, f32[704]{0:T(1024)S(1)} %get-tuple-element.8, ...), kind=kLoop, calls=%fused_computation.24 | loop fusion | flops 3244032 | bytes 1824768 | tf_op jit(solution)/shard_map/convert_element_type | solution.py:24
  146.6 0.0 all-gather.3.cloned.1.call-update
  146.6 0.0 all-reduce.4.cloned.1.call-start
  146.6 35.4 %all-gather.3.cloned.1.call-done = bf16[1024,704]{0,1:T(8,128)(2,1)} async-done(((bf16[256,704]{0,1:T(8,128)(2,1)}), bf16[1024,704]{0,1:T(8,128)(2,1)}) %all-gather.3.cloned.1.call-update) | async-done | bytes 1441808 | tf_op jit(solution)/shard_map/all_gather | solution.py:11
  182.1 1.5 copy.14
  183.5 5.4 %fusion.20 = f32[256,1024]{1,0:T(8,128)} fusion(bf16[256,2816]{0,1:T(8,128)(2,1)S(1)} %bitcast.11, bf16[2816,1024]{1,0:T(8,128)(2,1)} %param.18), kind=kOutput, calls=%fused_computation.36 | convolution fusion | flops 1476395008 | bytes 8257536 | tf_op jit(solution)/shard_map/dot_general | solution.py:60
  188.9 0.0 all-reduce.4.cloned.1.call-update
  188.9 34.6 %all-reduce.4.cloned.1.call-done = f32[256,1024]{1,0:T(8,128)} async-done(((f32[256,1024]{1,0:T(8,128)}), f32[256,1024]{1,0:T(8,128)}) %all-reduce.4.cloned.1.call-update) | async-done | bytes 1048592 | tf_op jit(solution)/shard_map/psum | solution.py:63
  223.6 1.5 multiply_reduce_fusion
  225.0 11.7 %psum.23 = f32[256]{0:T(256)S(1)} all-reduce(f32[256]{0:T(256)S(1)} %multiply_reduce_fusion), channel_id=1, replica_groups=mesh['grp'=2,'ra'=4,'cb'=4] {'ra'}, use_global_device_ids=true, to_apply=%region_6.7 | all-reduce | flops 256 | bytes 2048 | tf_op jit(solution)/shard_map/psum | solution.py:65
  236.7 2.2 multiply_convert_fusion
  (9 shorter events, 0.0 us)
Async XLA Ops:
  6.5 77.0 %reduce-scatter.5.cloned.1.call-start = ((), (), s32[]{:S(2)}) async-start(), calls=%async_computation.3 | async-start | bytes 3604480 | tf_op jit(solution)/shard_map/reduce_scatter | solution.py:48
  21.9 6.9 %copy-start = (bf16[256,1024]{1,0:T(8,128)(2,1)S(1)}, bf16[256,1024]{1,0:T(8,128)(2,1)}, u32[]{:S(2)}) copy-start(bf16[256,1024]{1,0:T(8,128)(2,1)} %param.10) | copy-start | bytes 1572868
  28.8 113.1 %reduce-scatter.3.cloned.1.call-start = ((), (), s32[]{:S(2)}) async-start(), calls=%async_computation.2 | async-start | bytes 3604480 | tf_op jit(solution)/shard_map/reduce_scatter | solution.py:47
  35.6 146.5 %all-gather.3.cloned.1.call-start = ((), (), s32[]{:S(2)}) async-start(), calls=%async_computation.5 | async-start | bytes 1802240 | tf_op jit(solution)/shard_map/all_gather | solution.py:11
  146.6 77.0 %all-reduce.4.cloned.1.call-start = ((), (), s32[]{:S(2)}) async-start(), calls=%async_computation.4 | async-start | bytes 2097152 | tf_op jit(solution)/shard_map/psum | solution.py:63
  183.5 5.4 %copy-start.1 = (bf16[1024]{0:T(1024)(128)(2,1)S(1)}, bf16[1024]{0:T(1024)(128)(2,1)}, u32[]{:S(2)}) copy-start(bf16[1024]{0:T(1024)(128)(2,1)} %param.19) | copy-start | bytes 6148
Sparse Core Ops, SparseCore 0:
  28.9 54.5 reduce-scatter.4
  85.8 56.0 reduce-scatter.2
  146.7 35.3 all-gather.2
  189.0 34.4 all-reduce.3
